TPU v7x, 32 devices: a whole 2x2x4 slice. The times are simulated.
32 devices in a mesh: sp: 16 (over z, y, x), tp: 2 (over core).
Axes of the slice: x: 2, y: 2, z: 4, core: 2. Of those that a mesh axis runs over, the one named last changes fastest.
Arguments:
- tokens: bfloat16 [8192, 4096], P(('sp', 'tp')), may hold values from -6 to 6
- norm_gain: float32 [4096], replicated, may hold values from 0.5 to 1.5
- query_weight: bfloat16 [4096, 1024], P(None, 'tp'), may hold values from -0.09375 to 0.09375
- key_weight: bfloat16 [4096, 1024], P(None, 'tp'), may hold values from -0.09375 to 0.09375
- value_weight: bfloat16 [4096, 2048], P(None, 'tp'), may hold values from -0.09375 to 0.09375
- gate_weight: bfloat16 [4096, 2048], P(None, 'tp'), may hold values from -0.09375 to 0.09375
- decay_bias: float32 [1024], P('tp'), may hold values from -0.5 to 0.5
- head_gain: float32 [2048], P('tp'), may hold values from 0.5 to 1.5
- out_weight: bfloat16 [2048, 4096], P('tp'), may hold values from -0.125 to 0.125
Outputs:
- layer_out: bfloat16 [8192, 4096], P(('sp', 'tp'))
All inputs are finite; a program needn't handle non-finite values.
Results may differ from a plain program's by a relative error of at most 0.015.
Values may be sent and summed in bfloat16 or wider, within the bound.
A program may use at most 192 MiB of HBM per device.

v0:
```python
import math

import jax
import jax.numpy as jnp
from jax import lax
from jax.sharding import PartitionSpec as P

HEAD_K = 128
HEAD_V = 256
BLOCK = 64


epsilon = 1e-06
decay_power = 16.0
precise = lax.Precision.HIGHEST


def gathered_then(shard, axis, dim, work):
    return work(lax.all_gather(shard, axis, axis=dim, tiled=True), jnp.int32(0))


def prefix(part, axis, combine, identity, reverse):
    count = lax.axis_size(axis)
    place = lax.axis_index(axis)
    ahead = count - 1 - place if reverse else place
    gathered = jax.tree.map(lambda a: lax.all_gather(a, axis), part)
    state = jax.tree.map(lambda a, e: jnp.zeros_like(a) + jnp.asarray(e, a.dtype), part, identity)

    def one(lap, state):
        source = count - 1 - lap if reverse else lap
        return combine(
            state, jax.tree.map(lambda a: lax.dynamic_index_in_dim(a, source, 0, False), gathered)
        )

    return lax.fori_loop(0, ahead, one, state)


def own_rows(portion, extent, axis):
    count = extent * lax.axis_size(axis)
    sent = portion(jnp.int32(0), count).astype(jnp.bfloat16)
    return lax.psum_scatter(sent, axis, scatter_dimension=0, tiled=True).astype(jnp.float32)


def to_blocks(values, head_width):
    block_count = values.shape[0] // BLOCK
    head_count = values.shape[1] // head_width
    return (
        values.astype(jnp.float32)
        .reshape(block_count, BLOCK, head_count, head_width)
        .transpose(2, 0, 1, 3)
    )


def combine(earlier_part, later_part):
    return (
        earlier_part[0] * later_part[0],
        later_part[0][..., None] * earlier_part[1] + later_part[1],
    )


def local_pass(queries, key_rows, value_rows, within, totals, start_state):
    block_end = totals[:, :, None, :]
    query_in = queries * jnp.exp(within)
    key_in = key_rows * jnp.exp(-within)
    key_out = key_rows * jnp.exp(block_end - within)
    causal = jnp.tril(jnp.ones((BLOCK, BLOCK), dtype=bool))
    scores = jnp.where(
        causal, jnp.einsum("hnid,hnjd->hnij", query_in, key_in, precision=precise), 0.0
    )
    local_out = jnp.einsum("hnij,hnjv->hniv", scores, value_rows, precision=precise)
    block_decay = jnp.exp(totals)

    def advance(carry_state, inputs_now):
        query_now, key_now, value_now, decay_now = inputs_now
        carried = jnp.einsum("hid,hdv->hiv", query_now, carry_state, precision=precise)
        carry_state = decay_now[..., None] * carry_state + jnp.einsum(
            "hjd,hjv->hdv", key_now, value_now, precision=precise
        )
        return (carry_state, carried)

    sequence_inputs = (
        jnp.moveaxis(query_in, 1, 0),
        jnp.moveaxis(key_out, 1, 0),
        jnp.moveaxis(value_rows, 1, 0),
        jnp.moveaxis(block_decay, 1, 0),
    )
    final_state, carried_out = lax.scan(advance, start_state, sequence_inputs)
    return (local_out + jnp.moveaxis(carried_out, 0, 1), final_state)


def mix_heads(queries, key_rows, value_rows, log_decay, carry):
    within = jnp.cumsum(log_decay, axis=2)
    totals = within[:, :, -1, :]
    before = jnp.cumsum(totals, axis=1) - totals
    span_end = before[:, -1, :] + totals[:, -1, :]
    through = within + before[:, :, None, :]
    key_out = key_rows * jnp.exp(span_end[:, None, None, :] - through)
    state_here = jnp.einsum("hncd,hncv->hdv", key_out, value_rows, precision=precise)
    carried_in = carry(jnp.exp(span_end), state_here)
    mixed_out, final_state = local_pass(queries, key_rows, value_rows, within, totals, carried_in)
    return mixed_out


def per_device(
    tokens,
    norm_gain,
    query_weight,
    key_weight,
    value_weight,
    gate_weight,
    decay_bias,
    head_gain,
    out_weight,
):
    inputs = tokens.astype(jnp.float32)
    row_scale = lax.rsqrt(jnp.mean(inputs * inputs, axis=-1, keepdims=True) + epsilon)
    normed = (inputs * row_scale * norm_gain.astype(jnp.float32)).astype(jnp.bfloat16)
    weights = (query_weight, key_weight, value_weight, gate_weight)

    def project(row_piece, row_start):
        return jnp.concatenate(
            [
                jnp.dot(row_piece, matrix, preferred_element_type=jnp.float32).astype(jnp.bfloat16)
                for matrix in weights
            ],
            axis=1,
        )

    projected = gathered_then(normed, "tp", 0, project)
    key_width = query_weight.shape[1]
    value_width = value_weight.shape[1]
    query_flat = projected[:, :key_width]
    key_flat = projected[:, key_width : 2 * key_width]
    value_flat = projected[:, 2 * key_width : 2 * key_width + value_width]
    gate_input = projected[:, 2 * key_width + value_width : 2 * key_width + 2 * value_width]
    span_rows = projected.shape[0]
    sequence = lax.axis_size("sp") * span_rows
    logits = decay_bias.astype(jnp.float32) + math.log(sequence / 8.0)
    log_decay = jnp.broadcast_to(jax.nn.log_sigmoid(logits) / decay_power, (span_rows, key_width))
    queries = to_blocks(query_flat, HEAD_K) * HEAD_K ** (-0.5)
    key_blocks = to_blocks(key_flat, HEAD_K)
    value_blocks = to_blocks(value_flat, HEAD_V)
    decay_blocks = to_blocks(log_decay, HEAD_K)
    head_count = queries.shape[0]

    def carry_all(span_decay, span_state):
        return prefix(
            (span_decay, span_state),
            "sp",
            combine,
            (jnp.ones_like(span_decay), jnp.zeros_like(span_state)),
            False,
        )[1]

    mixed_heads = mix_heads(queries, key_blocks, value_blocks, decay_blocks, carry_all)
    mixed_heads = mixed_heads.transpose(1, 2, 0, 3).reshape(span_rows, head_count, HEAD_V)
    head_scale = lax.rsqrt(jnp.mean(mixed_heads * mixed_heads, axis=-1, keepdims=True) + epsilon)
    normed_heads = (
        mixed_heads * head_scale * head_gain.astype(jnp.float32).reshape(head_count, HEAD_V)
    ).reshape(span_rows, head_count * HEAD_V)
    gated_rows = (normed_heads * jax.nn.silu(gate_input.astype(jnp.float32))).astype(jnp.bfloat16)
    rows_here = tokens.shape[0]

    def project_out(first_row, row_count):
        return jnp.dot(
            lax.dynamic_slice_in_dim(gated_rows, first_row, row_count, 0),
            out_weight,
            preferred_element_type=jnp.float32,
        )

    summed = own_rows(project_out, rows_here, "tp")
    return summed.astype(jnp.bfloat16)


def solution(mesh):
    return jax.shard_map(
        per_device,
        mesh=mesh,
        in_specs=(
            P(("sp", "tp"), None),
            P(),
            P(None, "tp"),
            P(None, "tp"),
            P(None, "tp"),
            P(None, "tp"),
            P("tp"),
            P("tp"),
            P("tp", None),
        ),
        out_specs=P(("sp", "tp"), None),
        check_vma=False,
    )
```

profile of v0, /device:TPU:24, one launch (start us, length us, event | category | flops | bytes accessed | tf_op | source)
XLA Modules:
  0.0 271.6 jit_solution(873285540672527308)
XLA Ops:
  6.5 2.1 fusion.4
  8.6 3.5 %fusion.6 = bf16[256,4096]{1,0:T(8,128)(2,1)} fusion(bf16[256,4096]{1,0:T(8,128)(2,1)} %param.13, f32[4096]{0:T(1024)} %param.14, f32[256]{0:T(256)S(1)} %add_rsqrt_fusion.1), kind=kLoop, calls=%fused_computation.16 | loop fusion | flops 4194304 | bytes 4211712 | tf_op jit(solution)/shard_map/convert_element_type | solution.py:117
  12.3 15.0 %all-gather.5.cloned.1.call-done = bf16[512,4096]{1,0:T(8,128)(2,1)} async-done(((bf16[256,4096]{1,0:T(8,128)(2,1)}), bf16[512,4096]{1,0:T(8,128)(2,1)}) %all-gather.5.cloned.1.call-update) | async-done | bytes 4194320 | tf_op jit(solution)/shard_map/all_gather | solution.py:19
  27.3 5.8 %fusion.12 = f32[512,512]{1,0:T(8,128)S(1)} fusion(bf16[512,4096]{1,0:T(8,128)(2,1)} %all-gather.5.cloned.1.call-done, bf16[4096,512]{1,0:T(8,128)(2,1)} %param.16), kind=kOutput, calls=%fused_computation.31 | convolution fusion | flops 2148007936 | bytes 9437184 | tf_op jit(solution)/shard_map/dot_general | solution.py:123
  33.4 5.8 %fusion.14 = f32[512,512]{1,0:T(8,128)S(1)} fusion(bf16[512,4096]{1,0:T(8,128)(2,1)} %all-gather.5.cloned.1.call-done, bf16[4096,512]{1,0:T(8,128)(2,1)} %param.15), kind=kOutput, calls=%fused_computation.34 | convolution fusion | flops 2148270080 | bytes 9437184 | tf_op jit(solution)/shard_map/dot_general | solution.py:123
  39.6 2.6 bitcast_multiply_fusion.4
  42.3 10.1 %convolution_convert_fusion.2 = bf16[512,1024]{1,0:T(8,128)(2,1)} fusion(bf16[512,4096]{1,0:T(8,128)(2,1)} %all-gather.5.cloned.1.call-done, bf16[4096,1024]{1,0:T(8,128)(2,1)} %param.17), kind=kOutput, calls=%fused_computation.28 | convolution fusion | flops 4295491584 | bytes 13631488 | tf_op jit(solution)/shard_map/dot_general | solution.py:123
  52.4 1.9 reshape.94
  54.3 3.4 %convolution_bitcast_fusion.1 = f32[4,128,256]{2,1,0:T(8,128)} fusion(bf16[8,64,4,256]{3,2,1,0:T(4,128)(2,1)S(1)} %reshape.94, f32[4,8,64,128]{3,1,2,0:T(8,128)S(1)} %get-tuple-element.143, f32[8,64,4,128]{3,2,1,0:T(4,128)S(1)} %reshape.97, f32[4,8,128]{2,1,0:T(8,128)S(1)} %get-tuple-element.142, f32[4,128]{1,0:T(4,128)S(1)} %bitcast.136), kind=kOutput, calls=%fused_computation.35 | convolution fusion | flops 806092800 | bytes 3688448 | tf_op jit(solution)/shard_map/hncd,hncv->hdv/dot_general | solution.py:98
  57.8 33.0 %all-gather = f32[64,1,128]{2,1,0:T(1,128)S(1)} all-gather(f32[4,1,128]{2,1,0:T(1,128)S(1)} %get-tuple-element.133), channel_id=2, replica_groups=mesh['sp'=16,'tp'=2] {'sp'}, dimensions={0}, use_global_device_ids=true | all-gather | bytes 34816 | tf_op jit(solution)/shard_map/all_gather | solution.py:26
  92.4 4.5 %convolution_select_fusion = f32[4,8,64,64]{3,2,1,0:T(8,128)} fusion(f32[4,8,64,128]{3,1,2,0:T(8,128)} %get-tuple-element.138, f32[4,8,64,128]{3,1,2,0:T(8,128)} %get-tuple-element.137, pred[64,64]{1,0:T(8,128)(4,1)S(1)} %iota_compare_fusion), kind=kOutput, calls=%fused_computation.29 | convolution fusion | flops 201457664 | bytes 2625536 | tf_op jit(solution)/shard_map/hnid,hnjd->hnij/dot_general | solution.py:68
  96.9 2.6 bitcast_multiply_fusion
  99.5 69.9 %all-gather.7.cloned.1.call-done = f32[64,128,256]{2,1,0:T(8,128)} async-done(((f32[4,128,256]{2,1,0:T(8,128)}), f32[64,128,256]{2,1,0:T(8,128)}) %all-gather.7.cloned.1.call-update) | async-done | bytes 8388624 | tf_op jit(solution)/shard_map/all_gather | solution.py:26
  169.4 15.0 %while.24 = (s32[]{:T(128)}, f32[4,128,256]{2,1,0:T(8,128)S(1)}, s32[]{:T(128)}, f32[16,4,128]{2,1,0:T(4,128)S(1)}, f32[16,4,128,256]{3,2,1,0:T(8,128)}, /*index=5*/s32[]{:T(128)}, s32[]{:T(128)}, s32[]{:T(128)}) while((s32[]{:T(128)}, f32[4,128,256]{2,1,0:T(8,128)S(1)}, s32[]{:T(128)}, f32[16,4,128]{2,1,0:T(4,128)S(1)}, ...), condition=%wide.region_4.5_spmd, body=%wide.region_3.4_spmd.sunk | while | flops 262149 | bytes 1579135 | solution.py:35
  184.4 36.9 %while.25 = (s32[]{:T(128)}, f32[4,128,256]{2,1,0:T(8,128)S(1)}, f32[8,4,64,256]{3,2,0,1:T(8,128)}, f32[8,4,128]{2,0,1:T(8,128)S(1)}, f32[8,4,64,128]{3,0,2,1:T(...) while((s32[]{:T(128)}, f32[4,128,256]{2,1,0:T(8,128)S(1)}, ...), condition=%wide.region_6.7_spmd, body=%wide.region_5.6_spmd.sunk | while | flops 201588736 | bytes 2890845 | solution.py:87
  184.5 1.8 constant_dynamic-slice_fusion.5
  189.1 1.7 constant_dynamic-slice_fusion.5
  192.0 1.7 convolution_add_fusion.2
  193.7 1.7 constant_dynamic-slice_fusion.5
  196.6 1.7 convolution_add_fusion.2
  198.4 1.7 constant_dynamic-slice_fusion.5
  201.2 1.7 convolution_add_fusion.2
  203.0 1.7 constant_dynamic-slice_fusion.5
  207.6 1.7 constant_dynamic-slice_fusion.5
  212.2 1.7 constant_dynamic-slice_fusion.5
  215.0 1.7 convolution_add_fusion.2
  216.8 1.7 constant_dynamic-slice_fusion.5
  221.4 4.1 %multiply_reduce_fusion = (f32[8,64,4]{1,0,2:T(8,128)S(1)}, f32[8,64,4,256]{3,1,0,2:T(8,128)}) fusion(f32[8,4,64,256]{3,2,0,1:T(8,128)} %get-tuple-element.87, f32[4,8,64,64]{3,2,1,0:T(8,128)S(1)} %copy-done.3, bf16[8,64,4,256]{3,2,1,0:T(4,128)(2,1)S(1)} %reshape.94), kind=kOutput, calls=%fused_computation.25 | convolution fusion | flops 404224000 | bytes 5775360 | tf_op jit(solution)/shard_map/hnij,hnjv->hniv/dot_general | solution.py:70
  226.2 1.8 copy.61
  229.4 1.8 copy.60
  231.3 17.4 %convolution_convert_fusion = bf16[512,4096]{1,0:T(8,128)(2,1)} fusion(bf16[1024,4096]{1,0:T(8,128)(2,1)} %param.21, f32[512,1024]{1,0:T(8,128)} %bitcast.131, f32[512,1024]{1,0:T(8,128)S(1)} %bitcast.130, bf16[512,4096]{1,0:T(8,128)(2,1)} %all-gather.5.cloned.1.call-done, bf16[4096,1024]{1,0:T(8,128)(2,1)} %param.18, f32[1024]{0:T(1024)S(1)} %copy-done.6), kind=kOutput, calls=%fused_computation.11 | convolution fusion | flops 8597274624 | bytes 29364224 | tf_op jit(solution)/shard_map/dot_general | solution.py:165
  248.8 16.3 %reduce-scatter.2.cloned.1.call-done = bf16[256,4096]{1,0:T(8,128)(2,1)} async-done(((bf16[512,4096]{1,0:T(8,128)(2,1)}), bf16[256,4096]{1,0:T(8,128)(2,1)}) %reduce-scatter.2.cloned.1.call-update) | async-done | bytes 2097168 | tf_op jit(solution)/shard_map/reduce_scatter | solution.py:41
  (81 shorter events, 35.2 us)
Async XLA Ops:
  6.5 5.7 %copy-start.5 = (f32[512]{0:T(512)S(1)}, f32[512]{0:T(512)}, u32[]{:S(2)}) copy-start(f32[512]{0:T(512)} %param.19) | copy-start | bytes 6148
  6.5 20.7 %all-gather.5.cloned.1.call-start = ((), (), s32[]{:S(2)}) async-start(), calls=%async_computation.1 | async-start | bytes 6291456 | tf_op jit(solution)/shard_map/all_gather | solution.py:19
  12.2 157.2 %all-gather.7.cloned.1.call-start = ((), (), s32[]{:S(2)}) async-start(), calls=%async_computation.3 | async-start | bytes 8912896 | tf_op jit(solution)/shard_map/all_gather | solution.py:26
  39.6 2.7 copy-start
  57.8 207.3 %reduce-scatter.2.cloned.1.call-start = ((), (), s32[]{:S(2)}) async-start(), calls=%async_computation.2 | async-start | bytes 6291456 | tf_op jit(solution)/shard_map/reduce_scatter | solution.py:41
  57.8 39.1 %copy-start.1 = (f32[8,64,4,128]{3,2,1,0:T(4,128)S(1)}, f32[8,64,4,128]{3,2,1,0:T(4,128)}, u32[]{:S(2)}) copy-start(f32[8,64,4,128]{3,2,1,0:T(4,128)} %copy-done) | copy-start | bytes 3145732
  184.4 36.9 %copy-start.3 = (f32[4,8,64,64]{3,2,1,0:T(8,128)S(1)}, f32[4,8,64,64]{3,2,1,0:T(8,128)}, u32[]{:S(2)}) copy-start(f32[4,8,64,64]{3,2,1,0:T(8,128)} %convolution_select_fusion) | copy-start | bytes 1572868
  225.4 2.6 copy-start.2
  228.0 3.2 %copy-start.6 = (f32[1024]{0:T(1024)S(1)}, f32[1024]{0:T(1024)}, u32[]{:S(2)}) copy-start(f32[1024]{0:T(1024)} %param.20) | copy-start | bytes 12292
  229.4 1.9 copy-start.4
Sparse Core Ops, SparseCore 0:
  12.3 14.8 all-gather.4
  57.9 111.4 all-gather.6
  248.9 16.1 reduce-scatter.1
where the time goes:
time: 274 us; the launch traced here: 272 us
  waiting for transfers between devices  101 us (37%)
  matrix products  73.7 us (27%)
  blocking collectives  33 us (12%)
  other arithmetic  27 us (10%)
  local copies, waits for them, and re-layouts  22.7 us (8%)
  between operations  13.3 us (5%)
    all_gather x1, waiting for transfers between devices, prefix(): gathered = jax.tree.map(lambda a: lax.all_gather(a, axis), part)  69.9 us
    all_gather x1, blocking collectives, prefix(): gathered = jax.tree.map(lambda a: lax.all_gather(a, axis), part)  33 us
    dot_general x3, matrix products, project(): jnp.dot(row_piece, matrix, preferred_element_type=jnp.float32)  21.7 us
    dot_general x1, matrix products, project_out(): jnp.dot(lax.dynamic_slice_in_dim(gated_rows, first_row, row_count, 0), ou...  17.4 us
    reduce_scatter x1, waiting for transfers between devices, own_rows(): lax.psum_scatter(sent, axis, scatter_dimension=0, tiled=True)  16.3 us
    all_gather x1, waiting for transfers between devices, gathered_then(): return work(lax.all_gather(shard, axis, axis=dim, tiled=True), jnp.int32(0))  15 us
    add x12, other arithmetic, combine(): later_part[0][..., None] * earlier_part[1] + later_part[1]  14.4 us
    dynamic_slice x16, local copies, waits for them, and re-layouts, local_pass(): final_state, carried_out = lax.scan(advance, start_state, sequence_inputs)  14.1 us
  transfers between devices with their start and end apart: 3, of which 3 were waited for; matrix products, arithmetic and copies ran while one was open for 3% of the time, Pallas kernels for 0%

commit v1 on v0

v1 whole, which is shorter than its diff:
```python
import functools
import math

import jax
import jax.numpy as jnp
from jax import lax
from jax.experimental import pallas as pl
from jax.experimental.pallas import tpu as pltpu
from jax.sharding import PartitionSpec as P

HEAD_K = 128
HEAD_V = 256

epsilon = 1e-06
decay_power = 16.0
MESH = pl.DeviceIdType.MESH
f32 = jnp.float32
bf16 = jnp.bfloat16
OUT_TILE = 512
VMEM_BYTES = 67_000_000


def nn(a, b):
    return jnp.dot(a, b, preferred_element_type=f32)


def nt(a, b):
    return lax.dot_general(a, b, (((1,), (1,)), ((), ())), preferred_element_type=f32)


def tn(a, b):
    return lax.dot_general(a, b, (((0,), (0,)), ((), ())), preferred_element_type=f32)


def kernel(
    sp_count,
    tokens,
    norm_gain,
    wq,
    wk,
    wv,
    wg,
    decay_bias,
    head_gain,
    wo,
    out,
    xn,
    w,
    wout,
    y,
    kin,
    qin,
    pv,
    gated,
    st_send,
    st_recv,
    tot_send,
    tot_recv,
    acc,
    c_send,
    c_recv,
    o_send,
    o_recv,
    o_buf,
    tok_sem,
    w_sem,
    wo_sem,
    tok_send,
    tok_recv,
    a_send,
    a_recv,
    b_send,
    b_recv,
    cs_send,
    cs_recv,
    os_send,
    os_recv,
    ob_sem,
):
    s = lax.axis_index("sp")
    c = lax.axis_index("tp")
    other = 1 - c
    half = tokens.shape[0]
    span = 2 * half
    width = wk.shape[1]
    heads = width // HEAD_K
    per = width // HEAD_V
    vtiles = wv.shape[1] // width
    inner = heads
    groups = sp_count // inner
    g = s // inner
    j = lax.rem(s, inner)

    own = pl.ds(pl.multiple_of(c * half, half), half)
    theirs = pl.ds(pl.multiple_of(other * half, half), half)

    def inner_dev(i):
        return {"sp": g * inner + i, "tp": c}

    def group_dev(k):
        return {"sp": k * inner + j, "tp": c}

    local_tok = pltpu.make_async_copy(tokens, xn.at[own], tok_sem)
    local_tok.start()
    sources = [wk.at[:, :]]
    sources += [wv.at[:, pl.ds(t * width, width)] for t in range(vtiles)]
    sources += [wq.at[:, :]]
    sources += [wg.at[:, pl.ds(t * width, width)] for t in range(vtiles)]
    count = len(sources)
    pltpu.make_async_copy(sources[0], w.at[0], w_sem.at[0]).start()

    barrier = pltpu.get_barrier_semaphore()
    pl.semaphore_signal(barrier, inc=1, device_id={"sp": s, "tp": other}, device_id_type=MESH)
    for d in range(1, inner):
        pl.semaphore_signal(
            barrier, inc=1, device_id=inner_dev(lax.rem(j + d, inner)), device_id_type=MESH
        )
    for d in range(1, groups):
        pl.semaphore_signal(
            barrier, inc=1, device_id=group_dev(lax.rem(g + d, groups)), device_id_type=MESH
        )
    pl.semaphore_wait(barrier, inner + groups - 1)

    send_tok = pltpu.make_async_remote_copy(
        src_ref=tokens,
        dst_ref=xn.at[own],
        send_sem=tok_send,
        recv_sem=tok_recv,
        device_id={"sp": s, "tp": other},
        device_id_type=MESH,
    )
    send_tok.start()
    for t in range(1, count):
        pltpu.make_async_copy(sources[t], w.at[t], w_sem.at[t]).start()
    wo_copy = pltpu.make_async_copy(wo, wout, wo_sem)
    wo_copy.start()

    chunk = 16

    def norm_rows(first):
        @pl.loop(0, half // chunk)
        def _(i):
            rows = pl.ds(pl.multiple_of(first + i * chunk, chunk), chunk)
            x = xn[rows, :].astype(f32)
            scale = lax.rsqrt(jnp.mean(x * x, axis=-1, keepdims=True) + epsilon)
            xn[rows, :] = (x * scale * norm_gain[...]).astype(bf16)

    def wait_w(t):
        pltpu.make_async_copy(wk, w.at[t], w_sem.at[t]).wait()

    local_tok.wait()
    norm_rows(c * half)
    wait_w(0)
    y[0, own, :] = nn(xn[own, :], w[0]).astype(bf16)
    send_tok.wait()
    norm_rows(other * half)
    y[0, theirs, :] = nn(xn[theirs, :], w[0]).astype(bf16)

    def project(t):
        wait_w(t)
        y[t] = nn(xn[...], w[t]).astype(bf16)

    @pl.loop(1, 1 + vtiles)
    def _(t):
        project(t)

    def log_decay_of(bias):
        return -jnp.log1p(jnp.exp(-(bias + math.log(sp_count * span / 8.0)))) / decay_power

    steps = (lax.broadcasted_iota(jnp.int32, (span, HEAD_K), 0) + 1).astype(f32)

    def column(row):
        half_tile = jnp.broadcast_to(row, (HEAD_K, HEAD_K)).T
        return jnp.concatenate([half_tile] * (HEAD_V // HEAD_K), axis=1)

    def value_of(h):
        return y[1 + h // per, :, pl.ds((h % per) * HEAD_V, HEAD_V)]

    for h in range(heads):
        keys = pl.ds(h * HEAD_K, HEAD_K)
        row = log_decay_of(decay_bias[pl.ds(h, 1), :])
        k_here = (y[0, :, keys].astype(f32) * jnp.exp(-row * steps)).astype(bf16)
        kin[:, keys] = k_here
        st_send[h] = (tn(k_here, value_of(h)) * column(jnp.exp(row * span))).astype(bf16)

    def copies(src, dst, ssem, rsem):
        made = []
        for d in range(1, inner):
            i = lax.rem(j + d, inner)
            made.append(
                pltpu.make_async_remote_copy(
                    src_ref=src.at[i],
                    dst_ref=dst.at[j],
                    send_sem=ssem.at[d - 1],
                    recv_sem=rsem.at[d - 1],
                    device_id=inner_dev(i),
                    device_id_type=MESH,
                )
            )
        return made

    a_copies = copies(st_send, st_recv, a_send, a_recv)
    for copy in a_copies:
        copy.start()
    st_recv[j] = st_send[j]

    @pl.loop(1 + vtiles, 3 + vtiles)
    def _(t):
        project(t)

    for copy in a_copies:
        copy.wait()
    mine = log_decay_of(decay_bias[pl.ds(j, 1), :])
    step_decay = column(jnp.exp(mine * span))
    total = st_recv[0].astype(f32)
    for i in range(1, inner):
        total = total * step_decay + st_recv[i].astype(f32)
    tot_send[...] = total.astype(bf16)

    def b_copy(d):
        return pltpu.make_async_remote_copy(
            src_ref=tot_send,
            dst_ref=tot_recv.at[d - 1],
            send_sem=b_send.at[d - 1],
            recv_sem=b_recv.at[d - 1],
            device_id=group_dev(lax.rem(g + d, groups)),
            device_id_type=MESH,
        )

    for d in range(1, groups):

        @pl.when(g + d < groups)
        def _():
            b_copy(d).start()

    @pl.loop(3 + vtiles, count)
    def _(t):
        project(t)

    for h in range(heads):
        keys = pl.ds(h * HEAD_K, HEAD_K)
        values = pl.ds(h * HEAD_V, HEAD_V)
        row = log_decay_of(decay_bias[pl.ds(h, 1), :])
        q_here = (
            y[1 + vtiles, :, keys].astype(f32) * (jnp.exp(row * steps) * HEAD_K ** (-0.5))
        ).astype(bf16)
        qin[:, keys] = q_here
        v_here = value_of(h)
        parts = 2
        rows = span // parts
        for p in range(parts):
            last = (p + 1) * rows
            scores = nt(q_here[p * rows : last], kin[pl.ds(0, last), keys])
            at = lax.broadcasted_iota(jnp.int32, scores.shape, 0) + p * rows
            to = lax.broadcasted_iota(jnp.int32, scores.shape, 1)
            scores = jnp.where(to <= at, scores, 0.0).astype(bf16)
            pv[pl.ds(p * rows, rows), values] = nn(scores, v_here[:last])

    acc[...] = jnp.zeros_like(acc)
    for d in range(1, groups):

        @pl.when(g >= d)
        def _():
            b_copy(d).wait_recv()
            far = column(jnp.exp(mine * (span * inner * (d - 1))))
            acc[...] += tot_recv[d - 1].astype(f32) * far

    carry = acc[...]
    c_send[0] = carry.astype(bf16)
    for i in range(1, inner):
        carry = carry * step_decay + st_recv[i - 1].astype(f32)
        c_send[i] = carry.astype(bf16)
    c_copies = copies(c_send, c_recv, cs_send, cs_recv)
    for copy in c_copies:
        copy.start()
    c_recv[j] = c_send[j]
    for copy in c_copies:
        copy.wait()

    for h in range(heads):
        keys = pl.ds(h * HEAD_K, HEAD_K)
        values = pl.ds(h * HEAD_V, HEAD_V)
        att = pv[:, values] + nn(qin[:, keys], c_recv[h])
        scale = lax.rsqrt(jnp.mean(att * att, axis=-1, keepdims=True) + epsilon)
        u = y[2 + vtiles + h // per, :, pl.ds((h % per) * HEAD_V, HEAD_V)].astype(f32)
        silu = u / (1.0 + jnp.exp(-u))
        gated[:, values] = (att * scale * head_gain[:, values] * silu).astype(bf16)

    tiles = wout.shape[1] // OUT_TILE

    def o_copy(t):
        return pltpu.make_async_remote_copy(
            src_ref=o_send.at[t],
            dst_ref=o_recv.at[t],
            send_sem=os_send.at[t],
            recv_sem=os_recv.at[t],
            device_id={"sp": s, "tp": other},
            device_id_type=MESH,
        )

    def out_copy(t):
        columns = pl.ds(pl.multiple_of(t * OUT_TILE, OUT_TILE), OUT_TILE)
        return pltpu.make_async_copy(o_buf.at[t], out.at[:, columns], ob_sem.at[t])

    wo_copy.wait()

    @pl.loop(0, tiles)
    def _(t):
        columns = pl.ds(pl.multiple_of(t * OUT_TILE, OUT_TILE), OUT_TILE)
        o_send[t] = nn(gated[theirs, :], wout[:, columns]).astype(bf16)
        o_copy(t).start()

    @pl.loop(0, tiles)
    def _(t):
        columns = pl.ds(pl.multiple_of(t * OUT_TILE, OUT_TILE), OUT_TILE)
        part = nn(gated[own, :], wout[:, columns])
        o_copy(t).wait()
        o_buf[t] = (part + o_recv[t].astype(f32)).astype(bf16)
        out_copy(t).start()

    @pl.loop(0, tiles)
    def _(t):
        out_copy(t).wait()

    for d in range(1, groups):

        @pl.when(g + d < groups)
        def _():
            b_copy(d).wait_send()


def per_device(sp_count, tokens, norm_gain, wq, wk, wv, wg, decay_bias, head_gain, wo):
    half, model = tokens.shape
    span = 2 * half
    width = wk.shape[1]
    vwidth = wv.shape[1]
    vtiles = vwidth // width
    heads = width // HEAD_K
    groups = sp_count // heads
    count = 2 + 2 * vtiles
    tiles = model // OUT_TILE
    state = (HEAD_K, HEAD_V)
    vm = pltpu.VMEM
    dma = pltpu.SemaphoreType.DMA
    hbm = pl.BlockSpec(memory_space=pltpu.HBM)
    vmem = pl.BlockSpec(memory_space=pltpu.VMEM)
    return pl.pallas_call(
        functools.partial(kernel, sp_count),
        out_shape=jax.ShapeDtypeStruct((half, model), bf16),
        in_specs=[hbm, vmem, hbm, hbm, hbm, hbm, vmem, vmem, hbm],
        out_specs=hbm,
        scratch_shapes=[
            vm((span, model), bf16),
            vm((count, model, width), bf16),
            vm((vwidth, model), bf16),
            vm((count, span, width), bf16),
            vm((span, width), bf16),
            vm((span, width), bf16),
            vm((span, vwidth), f32),
            vm((span, vwidth), bf16),
            vm((heads,) + state, bf16),
            vm((heads,) + state, bf16),
            vm(state, bf16),
            vm((groups,) + state, bf16),
            vm(state, f32),
            vm((heads,) + state, bf16),
            vm((heads,) + state, bf16),
            vm((tiles, half, OUT_TILE), bf16),
            vm((tiles, half, OUT_TILE), bf16),
            vm((tiles, half, OUT_TILE), bf16),
            dma,
            dma((count,)),
            dma,
            dma,
            dma,
            dma((heads,)),
            dma((heads,)),
            dma((groups,)),
            dma((groups,)),
            dma((heads,)),
            dma((heads,)),
            dma((tiles,)),
            dma((tiles,)),
            dma((tiles,)),
        ],
        compiler_params=pltpu.CompilerParams(
            collective_id=0, has_side_effects=True, vmem_limit_bytes=VMEM_BYTES
        ),
    )(
        tokens,
        norm_gain.reshape(1, model),
        wq,
        wk,
        wv,
        wg,
        decay_bias.reshape(heads, HEAD_K),
        head_gain.reshape(1, vwidth),
        wo,
    )


def solution(mesh):
    return jax.shard_map(
        functools.partial(per_device, mesh.shape["sp"]),
        mesh=mesh,
        in_specs=(
            P(("sp", "tp"), None),
            P(),
            P(None, "tp"),
            P(None, "tp"),
            P(None, "tp"),
            P(None, "tp"),
            P("tp"),
            P("tp"),
            P("tp", None),
        ),
        out_specs=P(("sp", "tp"), None),
        check_vma=False,
    )
```

time: 274 us -> 47.1 us (0.17)
  waiting for transfers between devices: 101 us -> 0 us
  matrix products: 73.7 us -> 0 us
  Pallas kernels: 0 us -> 43.8 us
  blocking collectives: 33 us -> 0 us
  other arithmetic: 27 us -> 0 us
  local copies, waits for them, and re-layouts: 22.7 us -> 3.13 us
  between operations: 13.3 us -> 0.01 us
    all_gather x2 -> x0, waiting for transfers between devices: 84.9 us -> none  [the longest x1 69.9 us: prefix(): gathered = jax.tree.map(lambda a: lax.all_gather(a, axis), part)]
    dot_general x23 -> x0, matrix products: 73.7 us -> none  [the longest x3 21.7 us: project(): jnp.dot(row_piece, matrix, preferred_element_type=jnp.float32)]
    pallas_call x0 -> x1, Pallas kernels: none -> 43.8 us  [per_device(): pl.pallas_call(functools.partial(kernel, sp_count), out_shape=jax.ShapeDt...]
    all_gather x1 -> x0, blocking collectives: 33 us -> none  [prefix(): gathered = jax.tree.map(lambda a: lax.all_gather(a, axis), part)]
    reduce_scatter x1 -> x0, waiting for transfers between devices: 16.3 us -> none  [own_rows(): lax.psum_scatter(sent, axis, scatter_dimension=0, tiled=True)]
    add x12 -> x0, other arithmetic: 14.4 us -> none  [combine(): later_part[0][..., None] * earlier_part[1] + later_part[1]]
    dynamic_slice x16 -> x0, local copies, waits for them, and re-layouts: 14.1 us -> none  [local_pass(): final_state, carried_out = lax.scan(advance, start_state, sequence_inputs)]
    another operation x3 -> x0, other arithmetic: 4.26 us -> none  [the longest x1 2.63 us: mix_heads(): within = jnp.cumsum(log_decay, axis=2)]
  transfers between devices with their start and end apart: 3 -> 0, of which waited for: 3 -> 0; matrix products, arithmetic and copies ran while one was open for 3% -> 0% of each run, Pallas kernels for 0% -> 0%
where the time goes in v1:
time: 47.1 us; the launch traced here: 46.9 us
  Pallas kernels  43.8 us (93%)
  local copies, waits for them, and re-layouts  3.13 us (7%)
    pallas_call x1, Pallas kernels, per_device(): pl.pallas_call(functools.partial(kernel, sp_count), out_shape=jax.ShapeDt...  43.8 us
    unnamed x1, local copies, waits for them, and re-layouts  3.13 us

profile of v1, /device:TPU:24, one launch (start us, length us, event | category | flops | bytes accessed | tf_op | source)
XLA Modules:
  0.0 46.9 jit_solution(4131926601721800222)
XLA Ops:
  0.0 43.8 %shard_map.91 = bf16[256,4096]{1,0:T(8,128)(2,1)} custom-call(bf16[256,4096]{1,0:T(8,128)(2,1)} %tokens.1, f32[1,4096]{1,0:T(1,128)} %bitcast.3, bf16[4096,512]{1,0:T(8,128)(2,1)} %wq.1, bf16[4096,512]{1,0:T(8,128)(2,1)} %wk.1, bf16[4096,1024]{1,0:T(8,128)(2,1)} %wv.1, bf16[4096,1024]{1,0:T(8,128)(2,1)} %wg.1, f32[4,128]{1,0:T(4,128)} %bitcast.5, ...), custom_call_target="tpu_custom_call" | custom-call | tf_op jit(solution)/shard_map/pallas_call | solution.py:347
  43.8 3.1 %copy.11 = bf16[256,4096]{1,0:T(8,128)(2,1)} copy(bf16[256,4096]{1,0:T(8,128)(2,1)} %shard_map.91) | data formatting | bytes 4194304

commit v2 on v1

--- a/solution.py
+++ b/solution.py
@@ -130,10 +130,9 @@
         device_id_type=MESH,
     )
     send_tok.start()
-    for t in range(1, count):
-        pltpu.make_async_copy(sources[t], w.at[t], w_sem.at[t]).start()
     wo_copy = pltpu.make_async_copy(wo, wout, wo_sem)
-    wo_copy.start()
+    fetches = [pltpu.make_async_copy(sources[t], w.at[t], w_sem.at[t]) for t in range(count)]
+    fetches.append(wo_copy)
 
     chunk = 16
 
@@ -149,8 +148,10 @@
         pltpu.make_async_copy(wk, w.at[t], w_sem.at[t]).wait()
 
     local_tok.wait()
+    fetches[1].start()
     norm_rows(c * half)
     wait_w(0)
+    fetches[2].start()
     y[0, own, :] = nn(xn[own, :], w[0]).astype(bf16)
     send_tok.wait()
     norm_rows(other * half)
@@ -158,6 +159,12 @@
 
     def project(t):
         wait_w(t)
+        for k in range(3, count + 1):
+
+            @pl.when(t + 2 == k)
+            def _():
+                fetches[k].start()
+
         y[t] = nn(xn[...], w[t]).astype(bf16)
 
     @pl.loop(1, 1 + vtiles)

time: 47.1 us -> 47.1 us (level)
  no operation moved by 1% of the time
where the time goes in v2:
time: 47.1 us; the launch traced here: 46.9 us
  Pallas kernels  43.8 us (93%)
  local copies, waits for them, and re-layouts  3.13 us (7%)
    pallas_call x1, Pallas kernels, per_device(): pl.pallas_call(functools.partial(kernel, sp_count), out_shape=jax.ShapeDt...  43.8 us
    unnamed x1, local copies, waits for them, and re-layouts  3.13 us

profile of v2, /device:TPU:24, one launch (start us, length us, event | category | flops | bytes accessed | tf_op | source)
XLA Modules:
  0.0 46.9 jit_solution(13280104934628568407)
XLA Ops:
  0.0 43.8 %shard_map.91 = bf16[256,4096]{1,0:T(8,128)(2,1)} custom-call(bf16[256,4096]{1,0:T(8,128)(2,1)} %tokens.1, f32[1,4096]{1,0:T(1,128)} %bitcast.3, bf16[4096,512]{1,0:T(8,128)(2,1)} %wq.1, bf16[4096,512]{1,0:T(8,128)(2,1)} %wk.1, bf16[4096,1024]{1,0:T(8,128)(2,1)} %wv.1, bf16[4096,1024]{1,0:T(8,128)(2,1)} %wg.1, f32[4,128]{1,0:T(4,128)} %bitcast.5, ...), custom_call_target="tpu_custom_call" | custom-call | tf_op jit(solution)/shard_map/pallas_call | solution.py:354
  43.8 3.1 %copy.11 = bf16[256,4096]{1,0:T(8,128)(2,1)} copy(bf16[256,4096]{1,0:T(8,128)(2,1)} %shard_map.91) | data formatting | bytes 4194304
